TPU v7x, 32 devices: a whole 2x2x4 slice. The times are simulated.
32 devices in a mesh: gr: 2 (over core), fs: 8 (over z, y), tp: 2 (over x).
Axes of the slice: x: 2, y: 2, z: 4, core: 2. Of those that a mesh axis runs over, the one named last changes fastest.
Arguments:
- tokens: bfloat16 [2048, 2048], P(('gr', 'fs')), may hold values from -6 to 6
- norm_gain: float32 [2048], P(('gr', 'fs')), may hold values from 0.1 to 1.9
- gate_train: float32 [32, 2048, 1024], P(None, ('gr', 'fs'), 'tp'), may hold values from -0.3125 to 0.3125
- up_train: float32 [32, 2048, 1024], P(None, ('gr', 'fs'), 'tp'), may hold values from -0.3125 to 0.3125
- down_train: float32 [32, 1024, 2048], P(None, ('gr', 'fs'), 'tp'), may hold values from -0.09375 to 0.09375
- routes: int32 [2048, 4], P(('gr', 'fs')), may hold values from 0 to 31, all different within a row; in each aligned block of 128 rows (0 to 127, 128 to 255, ...) at most 32 rows name the same one
- route_weight: float32 [2048, 4], P(('gr', 'fs')), may hold values from 0.05 to 1
Outputs:
- mixed: bfloat16 [2048, 2048], P(('gr', 'fs'), 'tp')
- gate_packed: bfloat16 [32, 2048, 1024], P('fs', None, 'tp')
- up_packed: bfloat16 [32, 2048, 1024], P('fs', None, 'tp')
- down_packed: bfloat16 [32, 1024, 2048], P('fs', 'tp')
Inputs may be any that keep to these rules, and one draw needn't show every extreme that they name: `routes`: each row names 4 different experts. Among the rows of one device no expert is named more than 32 times, and in every draw some expert is named exactly 32 times by the rows of some device.
All inputs are finite; a program needn't handle non-finite values.
Results may differ from a plain program's by a relative error of at most 0.015.
Values may be sent and summed in bfloat16 or wider, within the bound.
A program may use at most 128 MiB of HBM per device.

v0:
```python
import jax
import jax.numpy as jnp
from jax import lax
from jax.sharding import PartitionSpec as P

EXPERTS = 32
TOP = 4
CAP = 32


CLAMP_LIMIT = 7.0
SLOPE_ALPHA = 1.702
NORM_EPSILON = 1e-06


def body(tokens, norm_gain, gate_train, up_train, down_train, routes, route_weight):
    gate_local = (norm_gain[None, :, None] * gate_train).astype(jnp.bfloat16)
    up_local = (norm_gain[None, :, None] * up_train).astype(jnp.bfloat16)
    down_local = down_train.astype(jnp.bfloat16)
    served = (
        lax.all_to_all(gate_local, "fs", split_axis=0, concat_axis=1, tiled=True),
        lax.all_to_all(up_local, "fs", split_axis=0, concat_axis=1, tiled=True),
        lax.all_to_all(down_local, "fs", split_axis=0, concat_axis=1, tiled=True),
    )
    gate_weight, up_weight, down_cols = (
        lax.all_gather(served[0], "gr", axis=1, tiled=True),
        lax.all_gather(served[1], "gr", axis=1, tiled=True),
        lax.all_gather(served[2], "gr", axis=1, tiled=True),
    )
    down_weight = lax.all_to_all(down_cols, "tp", split_axis=1, concat_axis=2, tiled=True)
    tokens_wide = tokens.astype(jnp.float32)
    normed = (
        tokens_wide
        * lax.rsqrt(jnp.mean(tokens_wide * tokens_wide, axis=1, keepdims=True) + NORM_EPSILON)
    ).astype(jnp.bfloat16)
    flat_routes = routes.reshape(-1)
    one_hot = (flat_routes[:, None] == jnp.arange(EXPERTS, dtype=jnp.int32)[None, :]).astype(
        jnp.int32
    )
    counts = jnp.cumsum(one_hot, axis=0)
    slot_index = jnp.sum((counts - 1) * one_hot, axis=1)
    target_rows = flat_routes * CAP + slot_index
    copied_rows = jnp.repeat(normed, TOP, axis=0)
    dispatch_buffer = (
        jnp.zeros((EXPERTS * CAP, normed.shape[1]), jnp.bfloat16).at[target_rows].set(copied_rows)
    )
    dispatch_buffer = dispatch_buffer.reshape(EXPERTS, CAP, normed.shape[1])
    arrived = lax.all_to_all(dispatch_buffer, "fs", split_axis=0, concat_axis=1, tiled=True)
    gate_pre = jnp.einsum("erd,edf->erf", arrived, gate_weight, preferred_element_type=jnp.float32)
    up_pre = jnp.einsum("erd,edf->erf", arrived, up_weight, preferred_element_type=jnp.float32)
    clipped = jnp.minimum(gate_pre, CLAMP_LIMIT)
    hidden = (
        (jnp.clip(up_pre, -CLAMP_LIMIT, CLAMP_LIMIT) + 1.0)
        * clipped
        * jax.nn.sigmoid(SLOPE_ALPHA * clipped)
    ).astype(jnp.bfloat16)
    partial_value = jnp.einsum(
        "erf,efd->erd", hidden, down_weight, preferred_element_type=jnp.float32
    )
    summed = lax.psum_scatter(
        partial_value.astype(jnp.bfloat16), "tp", scatter_dimension=2, tiled=True
    )
    returned = lax.all_to_all(summed, "fs", split_axis=1, concat_axis=0, tiled=True)
    features = returned.shape[2]
    picked = (
        returned.reshape(EXPERTS * CAP, features)[target_rows]
        .reshape(tokens.shape[0], TOP, features)
        .astype(jnp.float32)
    )
    mixed = jnp.sum(picked * route_weight[:, :, None], axis=1).astype(jnp.bfloat16)
    return (mixed, gate_weight, up_weight, down_weight)


def solution(mesh):
    placed = (
        P(("gr", "fs"), None),
        P(("gr", "fs")),
        P(None, ("gr", "fs"), "tp"),
        P(None, ("gr", "fs"), "tp"),
        P(None, ("gr", "fs"), "tp"),
        P(("gr", "fs"), None),
        P(("gr", "fs"), None),
    )
    return jax.shard_map(
        body,
        mesh=mesh,
        in_specs=placed,
        out_specs=(
            P(("gr", "fs"), "tp"),
            P("fs", None, "tp"),
            P("fs", None, "tp"),
            P("fs", "tp", None),
        ),
        check_vma=False,
    )
```

profile of v0, /device:TPU:0, one launch (start us, length us, event | category | flops | bytes accessed | tf_op | source)
XLA Modules:
  0.0 677.3 jit_solution(9018972526156179878)
XLA Ops:
  7.2 6.1 convert_element_type.41
  13.2 7.4 %all-to-all-start.3 = ((bf16[32,64,1024]{2,1,0:T(8,128)(2,1)}), bf16[32,64,1024]{2,1,0:T(8,128)(2,1)}, u32[]{:S(2)}, u32[]{:S(2)}) async-start(bf16[32,64,1024]{2,1,0:T(8,128)(2,1)} %convert_element_type.41), calls=%async_computation.3 | async-start | bytes 8388608 | tf_op jit(solution)/shard_map/all_to_all | solution.py:23
  20.7 11.8 %multiply_convert_fusion.1 = (bf16[32,128,512]{2,1,0:T(8,128)(2,1)}, bf16[32,128,512]{2,1,0:T(8,128)(2,1)}) fusion(f32[32,128,512]{2,1,0:T(8,128)} %param.10, f32[128]{0:T(128)S(1)} %copy-done.4, f32[32,128,512]{2,1,0:T(8,128)} %param.9), kind=kLoop, calls=%fused_computation.3 | loop fusion | flops 8388608 | bytes 25166336 | tf_op jit(solution)/shard_map/convert_element_type | solution.py:18
  32.5 81.4 %all-to-all-done.3 = bf16[32,64,1024]{2,1,0:T(8,128)(2,1)} async-done(((bf16[32,64,1024]{2,1,0:T(8,128)(2,1)}), bf16[32,64,1024]{2,1,0:T(8,128)(2,1)}, u32[]{:S(2)}, u32[]{:S(2)}) %all-to-all-start.3) | async-done | bytes 4194336 | tf_op jit(solution)/shard_map/all_to_all | solution.py:23
  118.6 4.9 copy.43
  123.5 87.6 %all-to-all-done.2 = bf16[32,128,512]{2,1,0:T(8,128)(2,1)} async-done(((bf16[32,128,512]{2,1,0:T(8,128)(2,1)}), bf16[32,128,512]{2,1,0:T(8,128)(2,1)}, u32[]{:S(2)}, u32[]{:S(2)}) %all-to-all-start.2) | async-done | bytes 4194336 | tf_op jit(solution)/shard_map/all_to_all | solution.py:21
  215.7 4.6 copy.42
  226.6 7.8 %scatter_custom_fusion = bf16[1024,2048]{1,0:T(8,128)(2,1)} fusion(s32[512]{0:T(512)S(1)} %bitcast.59, bf16[512,2048]{1,0:T(8,128)(2,1)} %reshape.96, bf16[]{:T(256)} %constant.13.clone.1), kind=kCustom, calls=%fused_computation.7 | custom fusion | bytes 4194816 | tf_op jit(solution)/shard_map/scatter | solution.py:45
  234.4 73.8 %all-to-all-done.1 = bf16[32,128,512]{2,1,0:T(8,128)(2,1)} async-done(((bf16[32,128,512]{2,1,0:T(8,128)(2,1)}), bf16[32,128,512]{2,1,0:T(8,128)(2,1)}, u32[]{:S(2)}, u32[]{:S(2)}) %all-to-all-start.1) | async-done | bytes 4194336 | tf_op jit(solution)/shard_map/all_to_all | solution.py:22
  308.2 4.6 all-to-all-start
  317.4 12.1 %copy.44 = bf16[4,1024,1024]{2,0,1:T(4,128)(2,1)} copy(bf16[4,1024,1024]{2,1,0:T(8,128)(2,1)} %all-gather.8.cloned.1.call-done) | data formatting | bytes 16777216 | tf_op jit(solution)/shard_map/all_gather | solution.py:28
  329.6 75.7 %all-to-all-done = bf16[32,32,2048]{2,1,0:T(8,128)(2,1)} async-done(((bf16[32,32,2048]{2,1,0:T(8,128)(2,1)}), bf16[32,32,2048]{2,1,0:T(8,128)(2,1)}, u32[]{:S(2)}, u32[]{:S(2)}) %all-to-all-start) | async-done | bytes 4194336 | tf_op jit(solution)/shard_map/all_to_all | solution.py:48
  405.3 7.0 %all-to-all-start.4 = ((bf16[4,1024,1024]{2,0,1:T(4,128)(2,1)}), bf16[4,1024,1024]{2,0,1:T(4,128)(2,1)}, u32[]{:S(2)}, u32[]{:S(2)}) async-start(bf16[4,1024,1024]{2,0,1:T(4,128)(2,1)} %copy.44), calls=%async_computation.4 | async-start | bytes 16777216 | tf_op jit(solution)/shard_map/all_to_all | solution.py:30
  412.5 4.8 copy.40
  417.3 7.0 %fusion.11 = f32[4,256,512]{2,1,0:T(8,128)S(1)} fusion(bf16[4,256,2048]{2,1,0:T(8,128)(2,1)} %bitcast.57, bf16[4,2048,512]{2,1,0:T(8,128)(2,1)} %all-gather.6.cloned.1.call-done), kind=kOutput, calls=%fused_computation.29 | convolution fusion | flops 2147483648 | bytes 14680064 | tf_op jit(solution)/shard_map/erd,edf->erf/dot_general | solution.py:49
  424.3 78.9 %all-to-all-done.4 = bf16[4,1024,1024]{2,0,1:T(4,128)(2,1)} async-done(((bf16[4,1024,1024]{2,0,1:T(4,128)(2,1)}), bf16[4,1024,1024]{2,0,1:T(4,128)(2,1)}, u32[]{:S(2)}, u32[]{:S(2)}) %all-to-all-start.4) | async-done | bytes 8388640 | tf_op jit(solution)/shard_map/all_to_all | solution.py:30
  503.1 9.6 %copy.45 = bf16[4,1024,1024]{2,1,0:T(8,128)(2,1)} copy(bf16[4,1024,1024]{2,0,1:T(4,128)(2,1)} %all-to-all-done.4) | data formatting | bytes 16777216 | tf_op jit(solution)/shard_map/all_to_all | solution.py:30
  512.8 8.2 %copy.51 = bf16[4,2,64,8,1024]{4,3,1,2,0:T(8,128)(2,1)} copy(bf16[4,2,64,8,1024]{4,3,2,1,0:T(8,128)(2,1)} %bitcast.49) | data formatting | bytes 16777216 | tf_op jit(solution)/shard_map/all_to_all | solution.py:30
  521.0 13.9 %convolution_convert_fusion = bf16[4,256,2048]{2,1,0:T(8,128)(2,1)} fusion(bf16[4,512,2048]{2,1,0:T(8,128)(2,1)} %bitcast.54, f32[4,256,512]{2,1,0:T(8,128)S(1)} %fusion.11, bf16[4,256,2048]{2,1,0:T(8,128)(2,1)} %bitcast.58, bf16[4,2048,512]{2,1,0:T(8,128)(2,1)} %all-gather.4.cloned.1.call-done), kind=kOutput, calls=%fused_computation.4 | convolution fusion | flops 4302307328 | bytes 27262976 | tf_op jit(solution)/shard_map/erf,efd->erd/dot_general | solution.py:57
  535.0 54.6 %reduce-scatter.2.cloned.1.call-done = bf16[4,256,1024]{2,1,0:T(8,128)(2,1)} async-done(((bf16[4,256,2048]{2,1,0:T(8,128)(2,1)}), bf16[4,256,1024]{2,1,0:T(8,128)(2,1)}) %reduce-scatter.2.cloned.1.call-update) | async-done | bytes 2097168 | tf_op jit(solution)/shard_map/reduce_scatter | solution.py:60
  594.0 5.5 all-to-all-start.5
  599.7 47.9 %all-to-all-done.5 = bf16[4,256,1024]{2,0,1:T(4,128)(2,1)S(1)} async-done(((bf16[4,256,1024]{2,0,1:T(4,128)(2,1)}), bf16[4,256,1024]{2,0,1:T(4,128)(2,1)S(1)}, u32[]{:S(2)}, u32[]{:S(2)}) %all-to-all-start.5) | async-done | bytes 2097184 | tf_op jit(solution)/shard_map/all_to_all | solution.py:63
  656.1 7.3 %copy.55 = bf16[4,2048,512]{2,1,0:T(8,128)(2,1)} copy(bf16[4,2048,512]{2,1,0:T(8,128)(2,1)} %all-gather.6.cloned.1.call-done) | data formatting | bytes 16777216
  663.4 7.3 %copy.56 = bf16[4,2048,512]{2,1,0:T(8,128)(2,1)} copy(bf16[4,2048,512]{2,1,0:T(8,128)(2,1)} %all-gather.4.cloned.1.call-done) | data formatting | bytes 16777216
  (49 shorter events, 33.4 us)
Async XLA Ops:
  13.2 7.4 %copy-start.4 = (f32[128]{0:T(128)S(1)}, f32[128]{0:T(128)}, u32[]{:S(2)}) copy-start(f32[128]{0:T(128)} %param.8) | copy-start | bytes 1540
  13.2 100.7 %all-to-all-start.3 = ((bf16[32,64,1024]{2,1,0:T(8,128)(2,1)}), bf16[32,64,1024]{2,1,0:T(8,128)(2,1)}, u32[]{:S(2)}, u32[]{:S(2)}) async-start(bf16[32,64,1024]{2,1,0:T(8,128)(2,1)} %convert_element_type.41), calls=%async_computation.3 | async-start | bytes 8388608 | tf_op jit(solution)/shard_map/all_to_all | solution.py:23
  114.0 97.1 %all-to-all-start.2 = ((bf16[32,128,512]{2,1,0:T(8,128)(2,1)}), bf16[32,128,512]{2,1,0:T(8,128)(2,1)}, u32[]{:S(2)}, u32[]{:S(2)}) async-start(bf16[32,128,512]{2,1,0:T(8,128)(2,1)} %get-tuple-element.5), calls=%async_computation.2 | async-start | bytes 8388608 | tf_op jit(solution)/shard_map/all_to_all | solution.py:21
  118.5 198.9 %all-gather.8.cloned.1.call-start = ((), (), s32[]{:S(2)}) async-start(), calls=%async_computation.9 | async-start | bytes 12582912 | tf_op jit(solution)/shard_map/all_gather | solution.py:28
  211.1 97.1 %all-to-all-start.1 = ((bf16[32,128,512]{2,1,0:T(8,128)(2,1)}), bf16[32,128,512]{2,1,0:T(8,128)(2,1)}, u32[]{:S(2)}, u32[]{:S(2)}) async-start(bf16[32,128,512]{2,1,0:T(8,128)(2,1)} %get-tuple-element.4), calls=%async_computation.1 | async-start | bytes 8388608 | tf_op jit(solution)/shard_map/all_to_all | solution.py:22
  215.6 201.6 %all-gather.6.cloned.1.call-start = ((), (), s32[]{:S(2)}) async-start(), calls=%async_computation.8 | async-start | bytes 12582912 | tf_op jit(solution)/shard_map/all_gather | solution.py:26
  220.3 0.7 copy-start.2
  220.3 2.7 copy-start.1
  308.2 97.1 %all-to-all-start = ((bf16[32,32,2048]{2,1,0:T(8,128)(2,1)}), bf16[32,32,2048]{2,1,0:T(8,128)(2,1)}, u32[]{:S(2)}, u32[]{:S(2)}) async-start(bf16[32,32,2048]{2,1,0:T(8,128)(2,1)} %bitcast.53), calls=%async_computation | async-start | bytes 8388608 | tf_op jit(solution)/shard_map/all_to_all | solution.py:48
  312.8 208.2 %all-gather.4.cloned.1.call-start = ((), (), s32[]{:S(2)}) async-start(), calls=%async_computation.7 | async-start | bytes 12582912 | tf_op jit(solution)/shard_map/all_gather | solution.py:27
  405.3 97.8 %all-to-all-start.4 = ((bf16[4,1024,1024]{2,0,1:T(4,128)(2,1)}), bf16[4,1024,1024]{2,0,1:T(4,128)(2,1)}, u32[]{:S(2)}, u32[]{:S(2)}) async-start(bf16[4,1024,1024]{2,0,1:T(4,128)(2,1)} %copy.44), calls=%async_computation.4 | async-start | bytes 16777216 | tf_op jit(solution)/shard_map/all_to_all | solution.py:30
  412.3 177.2 %reduce-scatter.2.cloned.1.call-start = ((), (), s32[]{:S(2)}) async-start(), calls=%async_computation.10 | async-start | bytes 6291456 | tf_op jit(solution)/shard_map/reduce_scatter | solution.py:60
  535.0 64.6 %copy-start.3 = (f32[128,4]{0,1:T(4,128)S(1)}, f32[128,4]{0,1:T(4,128)}, u32[]{:S(2)}) copy-start(f32[128,4]{0,1:T(4,128)} %param.13) | copy-start | bytes 6148
  594.0 53.6 %all-to-all-start.5 = ((bf16[4,256,1024]{2,0,1:T(4,128)(2,1)}), bf16[4,256,1024]{2,0,1:T(4,128)(2,1)S(1)}, u32[]{:S(2)}, u32[]{:S(2)}) async-start(bf16[4,256,1024]{2,0,1:T(4,128)(2,1)} %copy.47), calls=%async_computation.6 | async-start | bytes 4194304 | tf_op jit(solution)/shard_map/all_to_all | solution.py:63
  647.6 1.3 copy-start
Sparse Core Ops, SparseCore 0:
  123.6 21.1 all-gather.7
  220.4 21.1 all-gather.5
  317.5 21.1 all-gather.3
  535.1 54.3 reduce-scatter.1
where the time goes:
time: 678 us; the launch traced here: 677 us
  waiting for transfers between devices  500 us (74%)
  local copies, waits for them, and re-layouts  86.9 us (13%)
  starting transfers between devices  34 us (5%)
  other arithmetic  21.7 us (3%)
  matrix products  20.9 us (3%)
  between operations  13.9 us (2%)
    all_to_all x1, waiting for transfers between devices, body(): lax.all_to_all(gate_local, 'fs', split_axis=0, concat_axis=1, tiled=True)  87.6 us
    all_to_all x1, waiting for transfers between devices, body(): lax.all_to_all(down_local, 'fs', split_axis=0, concat_axis=1, tiled=True)  81.4 us
    all_to_all x1, waiting for transfers between devices, body(): lax.all_to_all(down_cols, 'tp', split_axis=1, concat_axis=2, tiled=True)  78.9 us
    all_to_all x1, waiting for transfers between devices, body(): lax.all_to_all(dispatch_buffer, 'fs', split_axis=0, concat_axis=1, tiled=...  75.7 us
    all_to_all x1, waiting for transfers between devices, body(): lax.all_to_all(up_local, 'fs', split_axis=0, concat_axis=1, tiled=True)  73.8 us
    reduce_scatter x1, waiting for transfers between devices, body(): lax.psum_scatter(partial_value.astype(jnp.bfloat16), 'tp', scatter_dimens...  54.6 us
    all_to_all x1, waiting for transfers between devices, body(): lax.all_to_all(summed, 'fs', split_axis=1, concat_axis=0, tiled=True)  47.9 us
    all_to_all x2, local copies, waits for them, and re-layouts, body(): lax.all_to_all(down_cols, 'tp', split_axis=1, concat_axis=2, tiled=True)  17.9 us
  transfers between devices with their start and end apart: 10, of which 7 were waited for; matrix products, arithmetic and copies ran while one was open for 12% of the time, Pallas kernels for 0%

commit v1 on v0

v1 whole, which is shorter than its diff:
```python
import jax
import jax.numpy as jnp
from jax import lax
from jax.sharding import PartitionSpec as P

CAP = 32
CLAMP_LIMIT = 7.0
SLOPE_ALPHA = 1.702
NORM_EPSILON = 1e-06


def solution(mesh):
    gr_n, fs_n, tp_n = mesh.shape["gr"], mesh.shape["fs"], mesh.shape["tp"]

    def body(tokens, norm_gain, gate_train, up_train, down_train, routes, route_weight):
        experts = gate_train.shape[0]
        local_experts = experts // fs_n
        rows, width = tokens.shape
        gate_local = (norm_gain[None, :, None] * gate_train).astype(jnp.bfloat16)
        gate_part = lax.all_to_all(gate_local, "fs", split_axis=0, concat_axis=1, tiled=True)

        tokens_wide = tokens.astype(jnp.float32)
        normed = (
            tokens_wide
            * lax.rsqrt(jnp.mean(tokens_wide * tokens_wide, axis=1, keepdims=True) + NORM_EPSILON)
        ).astype(jnp.bfloat16)
        normed_all = lax.all_gather(normed, "fs", axis=0, tiled=False)
        routing = jnp.concatenate([routes.astype(jnp.float32), route_weight], axis=1)
        routing_all = lax.all_gather(routing, "fs", axis=0, tiled=False)
        top = routes.shape[1]
        routes_all = routing_all[:, :, :top].astype(jnp.int32)
        weight_all = routing_all[:, :, top:]
        mine = lax.axis_index("fs") * local_experts + jnp.arange(local_experts, dtype=jnp.int32)
        hit = routes_all[:, :, :, None] == mine[None, None, None, :]
        chosen = jnp.any(hit, axis=2)
        share = jnp.sum(jnp.where(hit, weight_all[:, :, :, None], 0.0), axis=2)
        lower = (jnp.arange(rows)[:, None] >= jnp.arange(rows)[None, :]).astype(jnp.bfloat16)
        count = jnp.einsum(
            "st,btj->bsj", lower, chosen.astype(jnp.bfloat16), preferred_element_type=jnp.float32
        )
        slot = jnp.where(chosen, count.astype(jnp.int32) - 1, -1)
        place = slot[:, :, :, None] == jnp.arange(CAP, dtype=jnp.int32)[None, None, None, :]
        pick = place.astype(jnp.bfloat16)
        spread = jnp.where(place, share[:, :, :, None], 0.0).astype(jnp.bfloat16)
        arrived = jnp.einsum(
            "btjc,btd->bjcd", pick, normed_all, preferred_element_type=jnp.float32
        ).astype(jnp.bfloat16)
        arrived = arrived.transpose(1, 0, 2, 3).reshape(local_experts, fs_n * CAP, width)

        gate_part, norm_gain, up_train = lax.optimization_barrier((gate_part, norm_gain, up_train))
        up_local = (norm_gain[None, :, None] * up_train).astype(jnp.bfloat16)
        up_part = lax.all_to_all(up_local, "fs", split_axis=0, concat_axis=1, tiled=True)
        gate_weight = lax.all_gather(gate_part, "gr", axis=1, tiled=True)
        up_part, down_train = lax.optimization_barrier((up_part, down_train))
        down_local = down_train.astype(jnp.bfloat16)
        down_part = lax.all_to_all(down_local, "fs", split_axis=0, concat_axis=1, tiled=True)
        up_weight = lax.all_gather(up_part, "gr", axis=1, tiled=True)

        gate_pre = jnp.einsum(
            "erd,edf->erf", arrived, gate_weight, preferred_element_type=jnp.float32
        )
        up_pre = jnp.einsum("erd,edf->erf", arrived, up_weight, preferred_element_type=jnp.float32)
        clipped = jnp.minimum(gate_pre, CLAMP_LIMIT)
        hidden = (
            (jnp.clip(up_pre, -CLAMP_LIMIT, CLAMP_LIMIT) + 1.0)
            * clipped
            * jax.nn.sigmoid(SLOPE_ALPHA * clipped)
        ).astype(jnp.bfloat16)
        hidden_all = lax.all_gather(hidden, "tp", axis=2, tiled=True)

        down_cols = lax.all_gather(down_part, "gr", axis=1, tiled=True)
        if gr_n == tp_n:
            swap = [(g * tp_n + t, t * tp_n + g) for g in range(gr_n) for t in range(tp_n)]
            turned = lax.ppermute(down_part, ("gr", "tp"), swap)
            down_weight = lax.all_gather(turned, "gr", axis=2, tiled=True)
        else:
            down_weight = lax.all_to_all(
                down_cols, "tp", split_axis=1, concat_axis=2, tiled=True
            )

        results = jnp.einsum(
            "erf,efd->erd", hidden_all, down_cols, preferred_element_type=jnp.float32
        ).astype(jnp.bfloat16)
        features = results.shape[2]
        results = results.reshape(local_experts, fs_n, CAP, features)
        partial_mix = jnp.einsum(
            "btjc,jbcd->btd", spread, results, preferred_element_type=jnp.float32
        ).astype(jnp.bfloat16)
        mixed = lax.psum_scatter(
            partial_mix.reshape(fs_n * rows, features), "fs", scatter_dimension=0, tiled=True
        )
        return (mixed, gate_weight, up_weight, down_weight)

    placed = (
        P(("gr", "fs"), None),
        P(("gr", "fs")),
        P(None, ("gr", "fs"), "tp"),
        P(None, ("gr", "fs"), "tp"),
        P(None, ("gr", "fs"), "tp"),
        P(("gr", "fs"), None),
        P(("gr", "fs"), None),
    )
    return jax.shard_map(
        body,
        mesh=mesh,
        in_specs=placed,
        out_specs=(
            P(("gr", "fs"), "tp"),
            P("fs", None, "tp"),
            P("fs", None, "tp"),
            P("fs", "tp", None),
        ),
        check_vma=False,
    )
```

time: 678 us -> 622 us (0.917)
  waiting for transfers between devices: 500 us -> 266 us
  blocking collectives: 0 us -> 209 us
  local copies, waits for them, and re-layouts: 86.9 us -> 38.1 us
  starting transfers between devices: 34 us -> 45.6 us
    all_to_all x4 -> x0, waiting for transfers between devices: 276 us -> none  [the longest x1 78.9 us: body(): lax.all_to_all(down_cols, 'tp', split_axis=1, concat_axis=2, tiled=True)]
    all_gather x0 -> x1, blocking collectives: none -> 112 us  [body(): routing_all = lax.all_gather(routing, 'fs', axis=0, tiled=False)]
    all_to_all x0 -> x1, blocking collectives: none -> 96.5 us  [body(): lax.all_to_all(up_local, 'fs', split_axis=0, concat_axis=1, tiled=True)]
    all_to_all x1, waiting for transfers between devices: 81.4 us -> 0.01 us  [body(): lax.all_to_all(down_local, 'fs', split_axis=0, concat_axis=1, tiled=True)]
    all_to_all x1, waiting for transfers between devices: 87.6 us -> 143 us  [body(): lax.all_to_all(gate_local, 'fs', split_axis=0, concat_axis=1, tiled=True)]
    all_gather x3 -> x6, waiting for transfers between devices: 0.02 us -> 50 us  [the longest x1 22.8 us: body(): down_weight = lax.all_gather(turned, 'gr', axis=2, tiled=True)]
    ppermute x0 -> x1, starting transfers between devices: none -> 32.9 us  [body(): turned = lax.ppermute(down_part, ('gr', 'tp'), swap)]
    all_to_all x4 -> x0, local copies, waits for them, and re-layouts: 25 us -> none  [the longest x2 17.9 us: body(): lax.all_to_all(down_cols, 'tp', split_axis=1, concat_axis=2, tiled=True)]
  transfers between devices with their start and end apart: 10 -> 10, of which waited for: 7 -> 5; matrix products, arithmetic and copies ran while one was open for 12% -> 9% of each run, Pallas kernels for 0% -> 0%
where the time goes in v1:
time: 622 us; the launch traced here: 619 us
  waiting for transfers between devices  266 us (43%)
  blocking collectives  209 us (34%)
  starting transfers between devices  45.6 us (7%)
  local copies, waits for them, and re-layouts  38.1 us (6%)
  matrix products  27.4 us (4%)
  other arithmetic  19.1 us (3%)
  between operations  14.3 us (2%)
    all_to_all x1, waiting for transfers between devices, body(): lax.all_to_all(gate_local, 'fs', split_axis=0, concat_axis=1, tiled=True)  143 us
    all_gather x1, blocking collectives, body(): routing_all = lax.all_gather(routing, 'fs', axis=0, tiled=False)  112 us
    all_to_all x1, blocking collectives, body(): lax.all_to_all(up_local, 'fs', split_axis=0, concat_axis=1, tiled=True)  96.5 us
    reduce_scatter x1, waiting for transfers between devices, body(): lax.psum_scatter(partial_mix.reshape(fs_n * rows, features), 'fs', scatte...  73.6 us
    ppermute x1, starting transfers between devices, body(): turned = lax.ppermute(down_part, ('gr', 'tp'), swap)  32.9 us
    unnamed x12, local copies, waits for them, and re-layouts  23.7 us
    all_gather x1, waiting for transfers between devices, body(): down_weight = lax.all_gather(turned, 'gr', axis=2, tiled=True)  22.8 us
    all_gather x1, waiting for transfers between devices, body(): down_cols = lax.all_gather(down_part, 'gr', axis=1, tiled=True)  22 us
  transfers between devices with their start and end apart: 10, of which 5 were waited for; matrix products, arithmetic and copies ran while one was open for 9% of the time, Pallas kernels for 0%

profile of v1, /device:TPU:0, one launch (start us, length us, event | category | flops | bytes accessed | tf_op | source)
XLA Modules:
  0.0 619.3 jit_solution(813496660095940591)
XLA Ops:
  7.2 6.8 %multiply_convert_fusion.1 = bf16[32,128,512]{2,1,0:T(8,128)(2,1)} fusion(f32[32,128,512]{2,1,0:T(8,128)} %param.9, f32[128]{0:T(128)} %param.8), kind=kLoop, calls=%fused_computation.1 | loop fusion | flops 4194304 | bytes 12583424 | tf_op jit(solution)/shard_map/convert_element_type | solution.py:19
  14.0 7.4 %all-to-all-start = ((bf16[32,128,512]{2,1,0:T(8,128)(2,1)}), bf16[32,128,512]{2,1,0:T(8,128)(2,1)}, u32[]{:S(2)}, u32[]{:S(2)}) async-start(bf16[32,128,512]{2,1,0:T(8,128)(2,1)} %multiply_convert_fusion.1), calls=%async_computation | async-start | bytes 8388608 | tf_op jit(solution)/shard_map/all_to_all | solution.py:20
  22.7 142.7 %all-to-all-done = bf16[32,128,512]{2,1,0:T(8,128)(2,1)} async-done(((bf16[32,128,512]{2,1,0:T(8,128)(2,1)}), bf16[32,128,512]{2,1,0:T(8,128)(2,1)}, u32[]{:S(2)}, u32[]{:S(2)}) %all-to-all-start) | async-done | bytes 4194336 | tf_op jit(solution)/shard_map/all_to_all | solution.py:20
  165.4 4.6 copy.31
  170.7 4.7 multiply_convert_fusion
  175.4 96.5 %all_to_all.54 = bf16[32,128,512]{2,1,0:T(8,128)(2,1)S(1)} all-to-all(bf16[32,128,512]{2,1,0:T(8,128)(2,1)S(1)} %multiply_convert_fusion), channel_id=1, replica_groups=mesh['gr'=2,'fs'=8,'tp'=2] {'fs'}, dimensions={0} | all-to-all | bytes 8388608 | tf_op jit(solution)/shard_map/all_to_all | solution.py:52
  271.9 2.5 copy.32
  274.4 6.2 convert_element_type.58
  280.6 4.8 all-to-all-start.2
  285.5 112.0 %all-gather = f32[1024,8]{0,1:T(8,128)S(1)} all-gather(f32[128,8]{0,1:T(8,128)S(1)} %pad_maximum_fusion), channel_id=2, replica_groups=mesh['gr'=2,'fs'=8,'tp'=2] {'fs'}, dimensions={0}, use_global_device_ids=true | all-gather | bytes 36864 | tf_op jit(solution)/shard_map/all_gather | solution.py:29
  397.8 3.4 convert_bitcast_fusion
  401.2 2.3 copy.30
  403.6 7.0 %fusion.15 = f32[4,256,512]{2,1,0:T(8,128)S(1)} fusion(bf16[4,256,2048]{2,1,0:T(8,128)(2,1)} %bitcast.48, bf16[4,2048,512]{2,1,0:T(8,128)(2,1)} %all-gather.11.cloned.1.call-done), kind=kOutput, calls=%fused_computation.32 | convolution fusion | flops 2147483648 | bytes 14680064 | tf_op jit(solution)/shard_map/erd,edf->erf/dot_general | solution.py:59
  410.6 8.4 %multiply_convert_fusion.2 = bf16[4,256,512]{2,1,0:T(8,128)(2,1)} fusion(f32[4,256,512]{2,1,0:T(8,128)S(1)} %fusion.15, bf16[4,256,2048]{2,1,0:T(8,128)(2,1)} %bitcast.49, bf16[4,2048,512]{2,1,0:T(8,128)(2,1)} %all-gather.9.cloned.1.call-done), kind=kOutput, calls=%fused_computation.5 | convolution fusion | flops 2152726528 | bytes 15728640 | tf_op jit(solution)/shard_map/erd,edf->erf/dot_general | solution.py:62
  419.1 4.9 copy.33
  424.1 32.9 %collective-permute-start = (bf16[4,512,1024]{2,1,0:T(8,128)(2,1)}, bf16[4,512,1024]{2,1,0:T(8,128)(2,1)}, u32[]{:S(2)}, u32[]{:S(2)}) collective-permute-start(bf16[4,512,1024]{2,1,0:T(8,128)(2,1)} %bitcast.44), channel_id=1, source_target_pairs={{0,0},{1,16},{16,1},{17,17},{2,2},{3,18},{18,3},{19,19},{4,4},{5,2... | collective-permute-start | bytes 12582920 | tf_op jit(solution)/shard_map/ppermute | solution.py:74
  457.3 5.2 all-gather.13.cloned.1.call-done
  462.5 22.0 %all-gather.15.cloned.1.call-done = bf16[4,1024,1024]{2,1,0:T(8,128)(2,1)} async-done(((bf16[4,512,1024]{2,1,0:T(8,128)(2,1)}), bf16[4,1024,1024]{2,1,0:T(8,128)(2,1)}) %all-gather.15.cloned.1.call-update) | async-done | bytes 8388624 | tf_op jit(solution)/shard_map/all_gather | solution.py:71
  484.5 6.4 %convolution_convert_fusion = bf16[4,256,1024]{2,1,0:T(8,128)(2,1)S(1)} fusion(bf16[4,256,1024]{2,1,0:T(8,128)(2,1)} %all-gather.13.cloned.1.call-done, bf16[4,1024,1024]{2,1,0:T(8,128)(2,1)} %all-gather.15.cloned.1.call-done), kind=kOutput, calls=%fused_computation.6 | convolution fusion | flops 2148532224 | bytes 12582912 | tf_op jit(solution)/shard_map/erf,efd->erd/dot_general | solution.py:81
  493.0 22.8 %all-gather.17.cloned.1.call-done = bf16[4,512,2048]{2,1,0:T(8,128)(2,1)} async-done(((bf16[4,512,1024]{2,1,0:T(8,128)(2,1)}), bf16[4,512,2048]{2,1,0:T(8,128)(2,1)}) %all-gather.17.cloned.1.call-update) | async-done | bytes 8388624 | tf_op jit(solution)/shard_map/all_gather | solution.py:75
  515.7 73.6 %reduce-scatter.2.cloned.1.call-done = bf16[128,1024]{1,0:T(8,128)(2,1)} async-done(((bf16[1024,1024]{1,0:T(8,128)(2,1)}), bf16[128,1024]{1,0:T(8,128)(2,1)}) %reduce-scatter.2.cloned.1.call-update) | async-done | bytes 262160 | tf_op jit(solution)/shard_map/reduce_scatter | solution.py:89
  589.4 7.3 %copy.45 = bf16[4,2048,512]{2,1,0:T(8,128)(2,1)} copy(bf16[4,2048,512]{2,1,0:T(8,128)(2,1)} %all-gather.11.cloned.1.call-done) | data formatting | bytes 16777216
  596.7 7.3 %copy.46 = bf16[4,2048,512]{2,1,0:T(8,128)(2,1)} copy(bf16[4,2048,512]{2,1,0:T(8,128)(2,1)} %all-gather.9.cloned.1.call-done) | data formatting | bytes 16777216
  604.0 8.4 %copy.47 = bf16[4,512,2048]{2,1,0:T(8,128)(2,1)} copy(bf16[4,512,2048]{2,1,0:T(8,128)(2,1)} %all-gather.17.cloned.1.call-done) | data formatting | bytes 16777216
  (42 shorter events, 4.9 us)
Async XLA Ops:
  14.0 7.5 %copy-start = (bf16[128,2048]{1,0:T(8,128)(2,1)S(1)}, bf16[128,2048]{1,0:T(8,128)(2,1)}, u32[]{:S(2)}) copy-start(bf16[128,2048]{1,0:T(8,128)(2,1)} %param.7) | copy-start | bytes 1572868
  14.0 151.5 %all-to-all-start = ((bf16[32,128,512]{2,1,0:T(8,128)(2,1)}), bf16[32,128,512]{2,1,0:T(8,128)(2,1)}, u32[]{:S(2)}, u32[]{:S(2)}) async-start(bf16[32,128,512]{2,1,0:T(8,128)(2,1)} %multiply_convert_fusion.1), calls=%async_computation | async-start | bytes 8388608 | tf_op jit(solution)/shard_map/all_to_all | solution.py:20
  21.4 376.4 %all-gather.19.cloned.1.call-start = ((), (), s32[]{:S(2)}) async-start(), calls=%async_computation.10 | async-start | bytes 4718592 | tf_op jit(solution)/shard_map/all_gather | solution.py:27
  22.7 380.9 %all-gather.11.cloned.1.call-start = ((), (), s32[]{:S(2)}) async-start(), calls=%async_computation.5 | async-start | bytes 12582912 | tf_op jit(solution)/shard_map/all_gather | solution.py:53
  170.0 0.7 copy-start.1
  170.1 240.5 %all-gather.9.cloned.1.call-start = ((), (), s32[]{:S(2)}) async-start(), calls=%async_computation.4 | async-start | bytes 12582912 | tf_op jit(solution)/shard_map/all_gather | solution.py:57
  280.6 4.8 copy-start.2
  280.6 4.9 copy-start.3
  280.6 138.4 %all-to-all-start.2 = ((bf16[32,64,1024]{2,1,0:T(8,128)(2,1)}), bf16[32,64,1024]{2,1,0:T(8,128)(2,1)}, u32[]{:S(2)}, u32[]{:S(2)}) async-start(bf16[32,64,1024]{2,1,0:T(8,128)(2,1)} %convert_element_type.58), calls=%async_computation.2 | async-start | bytes 8388608 | tf_op jit(solution)/shard_map/all_to_all | solution.py:56
  285.4 177.1 %all-gather.13.cloned.1.call-start = ((), (), s32[]{:S(2)}) async-start(), calls=%async_computation.6 | async-start | bytes 3145728 | tf_op jit(solution)/shard_map/all_gather | solution.py:69
  419.0 65.5 %all-gather.15.cloned.1.call-start = ((), (), s32[]{:S(2)}) async-start(), calls=%async_computation.7 | async-start | bytes 12582912 | tf_op jit(solution)/shard_map/all_gather | solution.py:71
  424.0 91.7 %all-gather.17.cloned.1.call-start = ((), (), s32[]{:S(2)}) async-start(), calls=%async_computation.9 | async-start | bytes 12582912 | tf_op jit(solution)/shard_map/all_gather | solution.py:75
  424.1 32.9 %collective-permute-start = (bf16[4,512,1024]{2,1,0:T(8,128)(2,1)}, bf16[4,512,1024]{2,1,0:T(8,128)(2,1)}, u32[]{:S(2)}, u32[]{:S(2)}) collective-permute-start(bf16[4,512,1024]{2,1,0:T(8,128)(2,1)} %bitcast.44), channel_id=1, source_target_pairs={{0,0},{1,16},{16,1},{17,17},{2,2},{3,18},{18,3},{19,19},{4,4},{5,2... | collective-permute-start | bytes 12582920 | tf_op jit(solution)/shard_map/ppermute | solution.py:74
  457.0 132.4 %reduce-scatter.2.cloned.1.call-start = ((), (), s32[]{:S(2)}) async-start(), calls=%async_computation.8 | async-start | bytes 2359296 | tf_op jit(solution)/shard_map/reduce_scatter | solution.py:89
Sparse Core Ops, SparseCore 0:
  24.3 136.8 all-gather.18
  170.2 18.6 all-gather.10
  274.6 18.8 all-gather.8
  419.1 43.3 all-gather.12
  464.5 19.9 all-gather.14
  485.9 29.7 all-gather.16
  519.8 69.4 reduce-scatter.1

commit v2 on v0

--- a/solution.py
+++ b/solution.py
@@ -1,19 +1,21 @@
 import jax
 import jax.numpy as jnp
 from jax import lax
+from jax.experimental import pallas as pl
+from jax.experimental.pallas import tpu as pltpu
 from jax.sharding import PartitionSpec as P
 
 EXPERTS = 32
 TOP = 4
 CAP = 32
-
-
 CLAMP_LIMIT = 7.0
 SLOPE_ALPHA = 1.702
 NORM_EPSILON = 1e-06
-
-
-def body(tokens, norm_gain, gate_train, up_train, down_train, routes, route_weight):
+MESH = pl.DeviceIdType.MESH
+STEPS = (2, 3, 1, 6, 7, 4, 5)
+
+
+def plain_body(tokens, norm_gain, gate_train, up_train, down_train, routes, route_weight):
     gate_local = (norm_gain[None, :, None] * gate_train).astype(jnp.bfloat16)
     up_local = (norm_gain[None, :, None] * up_train).astype(jnp.bfloat16)
     down_local = down_train.astype(jnp.bfloat16)
@@ -71,6 +73,334 @@
     return (mixed, gate_weight, up_weight, down_weight)
 
 
+def flip(fs, step):
+    z, y = lax.div(fs, 2), lax.rem(fs, 2)
+    if step % 2:
+        y = 1 - y
+    if step // 2 == 3:
+        z = 3 - z
+    elif step // 2 == 2:
+        z = lax.rem(z + 2, 4)
+    elif step // 2 == 1:
+        z = z + 1 - 2 * lax.rem(z, 2)
+    return z * 2 + y
+
+
+def exchange_kernel(
+    normed, routing, gate, up, down,
+    normed_all, routing_all, gate_out, up_out, down_out,
+    send, recv, relay_send, relay_recv, local_sem, tok_send, tok_recv, route_send, route_recv,
+):
+    g, f, t = lax.axis_index("gr"), lax.axis_index("fs"), lax.axis_index("tp")
+    local_experts = gate_out.shape[0]
+    fs_n = 8
+    rows, down_rows = gate.shape[1], down.shape[1]
+    wide = down.shape[2]
+    half = normed.shape[1] // 2
+
+    barrier = pltpu.get_barrier_semaphore()
+
+    def greet(device):
+        pl.semaphore_signal(barrier, inc=1, device_id=device, device_id_type=MESH)
+
+    for step in STEPS:
+        greet((g, flip(f, step), t))
+    for step in range(fs_n):
+        greet((1 - g, flip(f, step), 1 - t))
+    greet((1 - g, f, t))
+    greet((g, f, 1 - t))
+    pl.semaphore_wait(barrier, 17)
+
+    def remote(src, dst, s, r, device):
+        return pltpu.make_async_remote_copy(
+            src_ref=src, dst_ref=dst, send_sem=s, recv_sem=r, device_id=device, device_id_type=MESH
+        )
+
+    def tok(block):
+        return normed_all.at[block, :, pl.ds(pl.multiple_of(t * half, half), half)]
+
+    own_half = normed.at[:, pl.ds(pl.multiple_of(t * half, half), half)]
+    first = {s: remote(own_half, tok(f), tok_send.at[s], tok_recv.at[s], (g, flip(f, s), t))
+             for s in (2, 4, 6)}
+    for s in (6, 4, 2):
+        first[s].start()
+    small = {s: remote(routing, routing_all.at[f], route_send.at[s], route_recv.at[s],
+                       (g, flip(f, s), t)) for s in STEPS}
+    for s in STEPS:
+        small[s].start()
+
+    def gate_at(whole, group, owner):
+        return whole.at[:, pl.ds(pl.multiple_of((group * fs_n + owner) * rows, rows), rows), :]
+
+    def down_at(owner, group):
+        return down_out.at[
+            :,
+            pl.ds(pl.multiple_of(owner * down_rows, down_rows), down_rows),
+            pl.ds(pl.multiple_of(group * wide, wide), wide),
+        ]
+
+    def part(whole, owner):
+        return whole.at[pl.ds(owner * local_experts, local_experts)]
+
+    partner = (1 - g, f, t)
+    keep = [
+        pltpu.make_async_copy(part(gate, f), gate_at(gate_out, g, f), local_sem.at[0]),
+        pltpu.make_async_copy(part(up, f), gate_at(up_out, g, f), local_sem.at[1]),
+        pltpu.make_async_copy(normed, normed_all.at[f], local_sem.at[2]),
+        pltpu.make_async_copy(routing, routing_all.at[f], local_sem.at[3]),
+    ]
+    main = {}
+    for s in STEPS:
+        there = flip(f, s)
+        main[0, s] = remote(part(gate, there), gate_at(gate_out, g, f), send.at[0, s],
+                            recv.at[0, s], (g, there, t))
+        main[1, s] = remote(part(up, there), gate_at(up_out, g, f), send.at[1, s],
+                            recv.at[1, s], (g, there, t))
+        main[2, s] = remote(part(down, there), down_at(f, t), send.at[2, s], recv.at[2, s],
+                            (t, there, g))
+    turn = remote(part(down, f), down_at(f, t), send.at[2, 0], recv.at[2, 0], (1 - g, f, 1 - t))
+    stay = pltpu.make_async_copy(part(down, f), down_at(f, t), local_sem.at[4])
+
+    for s in STEPS:
+        for which in range(3):
+            main[which, s].start()
+
+    @pl.when(g != t)
+    def _():
+        turn.start()
+
+    @pl.when(g == t)
+    def _():
+        stay.start()
+
+    for copy in keep:
+        copy.start()
+
+    relays = {}
+    relays[0, 0] = remote(part(gate, f), gate_at(gate_out, g, f), relay_send.at[0, 0],
+                          relay_recv.at[0, 0], partner)
+    relays[1, 0] = remote(part(up, f), gate_at(up_out, g, f), relay_send.at[1, 0],
+                          relay_recv.at[1, 0], partner)
+    relays[0, 0].start()
+    relays[1, 0].start()
+
+    across = (g, flip(f, 1), t)
+    second = {0: remote(own_half, tok(f), tok_send.at[1], tok_recv.at[1], across)}
+    second[0].start()
+    for s in (2, 4, 6):
+        first[s].wait_recv()
+        second[s] = remote(tok(flip(f, s)), tok(flip(f, s)), tok_send.at[s + 1],
+                           tok_recv.at[s + 1], across)
+        second[s].start()
+    beside = (g, f, 1 - t)
+    third = {}
+    for s in (2, 4, 6, 1, 3, 5, 7):
+        if s % 2:
+            second[s - 1].wait_recv()
+        third[s] = remote(tok(flip(f, s)), tok(flip(f, s)), tok_send.at[8 + s],
+                          tok_recv.at[8 + s], beside)
+        third[s].start()
+
+    @pl.when(g != t)
+    def _():
+        turn.wait()
+
+    @pl.when(g == t)
+    def _():
+        stay.wait()
+
+    relays[2, 0] = remote(down_at(f, g), down_at(f, g), relay_send.at[2, 0],
+                          relay_recv.at[2, 0], partner)
+    relays[2, 0].start()
+    for s in STEPS:
+        source = flip(f, s)
+        for which in range(3):
+            main[which, s].wait_recv()
+            if which == 2:
+                block = down_at(source, g)
+            else:
+                block = gate_at((gate_out, up_out)[which], g, source)
+            relays[which, s] = remote(block, block, relay_send.at[which, s],
+                                      relay_recv.at[which, s], partner)
+            relays[which, s].start()
+    for s in (0,) + STEPS:
+        for which in range(3):
+            relays[which, s].wait()
+    for s in STEPS:
+        for which in range(3):
+            main[which, s].wait_send()
+        small[s].wait()
+        third[s].wait()
+    for s in (2, 4, 6):
+        first[s].wait_send()
+    for s in (0, 2, 4, 6):
+        second[s].wait_send()
+    for copy in keep:
+        copy.wait()
+
+
+def return_kernel(partial_mix, mixed, near, summed, far, send, recv, far_send, far_recv):
+    g, f, t = lax.axis_index("gr"), lax.axis_index("fs"), lax.axis_index("tp")
+    y = lax.rem(f, 2)
+    half = mixed.shape[1]
+    quad = ((0, 1), (1, 0), (1, 1))
+    barrier = pltpu.get_barrier_semaphore()
+    for dy, dx in quad:
+        device = (g, flip(f, dy), 1 - t if dx else t)
+        pl.semaphore_signal(barrier, inc=1, device_id=device, device_id_type=MESH)
+    for step in (2, 4, 6):
+        device = (g, flip(f, step), t)
+        pl.semaphore_signal(barrier, inc=1, device_id=device, device_id_type=MESH)
+    pl.semaphore_wait(barrier, 6)
+
+    steps = (6, 4, 2, 0)
+    copies = {}
+    for i, step in enumerate(steps):
+        for q, (dy, dx) in enumerate(quad):
+            there = flip(f, step + dy)
+            side = 1 - t if dx else t
+            copies[i, q] = pltpu.make_async_remote_copy(
+                src_ref=partial_mix.at[there, :, pl.ds(pl.multiple_of(side * half, half), half)],
+                dst_ref=near.at[i, q],
+                send_sem=send.at[i, q],
+                recv_sem=recv.at[i, q],
+                device_id=(g, flip(f, dy), side),
+                device_id_type=MESH,
+            )
+            copies[i, q].start()
+    onward = {}
+    for i, step in enumerate(steps):
+        for q in range(3):
+            copies[i, q].wait_recv()
+        there = flip(f, step)
+        own = partial_mix[there, :, pl.ds(pl.multiple_of(t * half, half), half)]
+        total = own.astype(jnp.float32)
+        for q in range(3):
+            total = total + near[i, q].astype(jnp.float32)
+        if step:
+            summed[i] = total.astype(jnp.bfloat16)
+            onward[i] = pltpu.make_async_remote_copy(
+                src_ref=summed.at[i],
+                dst_ref=far.at[i],
+                send_sem=far_send.at[i],
+                recv_sem=far_recv.at[i],
+                device_id=(g, there, t),
+                device_id_type=MESH,
+            )
+            onward[i].start()
+    for i in (2, 1, 0):
+        onward[i].wait_recv()
+        total = total + far[i].astype(jnp.float32)
+    mixed[...] = total.astype(jnp.bfloat16)
+    for i in range(3):
+        onward[i].wait_send()
+    for i in range(4):
+        for q in range(3):
+            copies[i, q].wait_send()
+
+
+def body(tokens, norm_gain, gate_train, up_train, down_train, routes, route_weight):
+    fs_n = 8
+    experts, rows_in, hidden_part = gate_train.shape
+    local_experts = experts // fs_n
+    rows, width = tokens.shape
+    top = routes.shape[1]
+    gate_local = (norm_gain[None, :, None] * gate_train).astype(jnp.bfloat16)
+    up_local = (norm_gain[None, :, None] * up_train).astype(jnp.bfloat16)
+    down_local = down_train.astype(jnp.bfloat16)
+    tokens_wide = tokens.astype(jnp.float32)
+    normed = (
+        tokens_wide
+        * lax.rsqrt(jnp.mean(tokens_wide * tokens_wide, axis=1, keepdims=True) + NORM_EPSILON)
+    ).astype(jnp.bfloat16)
+    routing = jnp.concatenate([routes.astype(jnp.float32).T, route_weight.T], axis=0)
+
+    anywhere = pl.BlockSpec(memory_space=pl.ANY)
+    dma = pltpu.SemaphoreType.DMA
+    normed_all, routing_all, gate_weight, up_weight, down_weight = pl.pallas_call(
+        exchange_kernel,
+        out_shape=(
+            jax.ShapeDtypeStruct((fs_n, rows, width), jnp.bfloat16),
+            jax.ShapeDtypeStruct((fs_n,) + routing.shape, jnp.float32),
+            jax.ShapeDtypeStruct((local_experts, rows_in * 2 * fs_n, hidden_part), jnp.bfloat16),
+            jax.ShapeDtypeStruct((local_experts, rows_in * 2 * fs_n, hidden_part), jnp.bfloat16),
+            jax.ShapeDtypeStruct(
+                (local_experts, down_train.shape[1] * fs_n, down_train.shape[2] * 2), jnp.bfloat16
+            ),
+        ),
+        in_specs=[anywhere] * 5,
+        out_specs=(anywhere,) * 5,
+        scratch_shapes=[
+            dma((3, 8)), dma((3, 8)), dma((3, 8)), dma((3, 8)), dma((5,)),
+            dma((16,)), dma((16,)), dma((8,)), dma((8,)),
+        ],
+        compiler_params=pltpu.CompilerParams(collective_id=0, has_side_effects=True),
+    )(normed, routing, gate_local, up_local, down_local)
+
+    routes_all = routing_all[:, :top].astype(jnp.int32)
+    weight_all = routing_all[:, top:]
+    mine = lax.axis_index("fs") * local_experts + jnp.arange(local_experts, dtype=jnp.int32)
+    hit = routes_all[:, None, :, :] == mine[None, :, None, None]
+    chosen = jnp.any(hit, axis=2)
+    share = jnp.sum(jnp.where(hit, weight_all[:, None, :, :], 0.0), axis=2)
+    lower = (jnp.arange(rows)[:, None] <= jnp.arange(rows)[None, :]).astype(jnp.bfloat16)
+    count = jnp.einsum(
+        "bjt,ts->bjs", chosen.astype(jnp.bfloat16), lower, preferred_element_type=jnp.float32
+    )
+    slot = jnp.where(chosen, count.astype(jnp.int32) - 1, -1)
+    place = slot[:, :, None, :] == jnp.arange(CAP, dtype=jnp.int32)[None, None, :, None]
+    pick = place.astype(jnp.bfloat16).reshape(fs_n, local_experts * CAP, rows)
+    spread = (
+        jnp.where(place, share[:, :, None, :], 0.0)
+        .astype(jnp.bfloat16)
+        .reshape(fs_n, local_experts * CAP, rows)
+    )
+    arrived = jnp.einsum(
+        "bst,btd->bsd", pick, normed_all, preferred_element_type=jnp.float32
+    ).astype(jnp.bfloat16)
+    arrived = (
+        arrived.reshape(fs_n, local_experts, CAP, width)
+        .transpose(1, 0, 2, 3)
+        .reshape(local_experts, fs_n * CAP, width)
+    )
+    gate_pre = jnp.einsum("erd,edf->erf", arrived, gate_weight, preferred_element_type=jnp.float32)
+    up_pre = jnp.einsum("erd,edf->erf", arrived, up_weight, preferred_element_type=jnp.float32)
+    clipped = jnp.minimum(gate_pre, CLAMP_LIMIT)
+    hidden = (
+        (jnp.clip(up_pre, -CLAMP_LIMIT, CLAMP_LIMIT) + 1.0)
+        * clipped
+        * jax.nn.sigmoid(SLOPE_ALPHA * clipped)
+    ).astype(jnp.bfloat16)
+    results = jnp.einsum(
+        "erf,efd->erd", hidden, down_weight, preferred_element_type=jnp.float32
+    ).astype(jnp.bfloat16)
+    results = (
+        results.reshape(local_experts, fs_n, CAP, width)
+        .transpose(1, 0, 2, 3)
+        .reshape(fs_n, local_experts * CAP, width)
+    )
+    partial_mix = jnp.einsum(
+        "bst,bsd->btd", spread, results, preferred_element_type=jnp.float32
+    ).astype(jnp.bfloat16)
+
+    in_vmem = pl.BlockSpec(memory_space=pltpu.VMEM)
+    half = width // 2
+    mixed = pl.pallas_call(
+        return_kernel,
+        out_shape=jax.ShapeDtypeStruct((rows, half), jnp.bfloat16),
+        in_specs=[in_vmem],
+        out_specs=in_vmem,
+        scratch_shapes=[
+            pltpu.VMEM((4, 3, rows, half), jnp.bfloat16),
+            pltpu.VMEM((3, rows, half), jnp.bfloat16),
+            pltpu.VMEM((3, rows, half), jnp.bfloat16),
+            dma((4, 3)), dma((4, 3)), dma((3,)), dma((3,)),
+        ],
+        compiler_params=pltpu.CompilerParams(collective_id=1, has_side_effects=True),
+    )(partial_mix)
+    return (mixed, gate_weight, up_weight, down_weight)
+
+
 def solution(mesh):
     placed = (
         P(("gr", "fs"), None),
@@ -81,8 +411,9 @@
         P(("gr", "fs"), None),
         P(("gr", "fs"), None),
     )
+    block = mesh.shape["gr"] == 2 and mesh.shape["fs"] == 8 and mesh.shape["tp"] == 2
     return jax.shard_map(
-        body,
+        body if block else plain_body,
         mesh=mesh,
         in_specs=placed,
         out_specs=(

time: 678 us -> 466 us (0.69)
  waiting for transfers between devices: 500 us -> 0 us
  Pallas kernels: 0 us -> 388 us
  local copies, waits for them, and re-layouts: 86.9 us -> 32.2 us
  starting transfers between devices: 34 us -> 0 us
  between operations: 13.9 us -> 0.77 us
    all_to_all x6 -> x0, waiting for transfers between devices: 445 us -> none  [the longest x1 87.6 us: body(): lax.all_to_all(gate_local, 'fs', split_axis=0, concat_axis=1, tiled=True)]
    pallas_call x0 -> x2, Pallas kernels: none -> 388 us  [the longest x1 335 us: body(): pl.pallas_call(exchange_kernel, out_shape=(jax.ShapeDtypeStruct((fs_n, ro...]
    reduce_scatter x1 -> x0, waiting for transfers between devices: 54.6 us -> none  [body(): lax.psum_scatter(partial_value.astype(jnp.bfloat16), 'tp', scatter_dimens...]
    all_to_all x7 -> x0, local copies, waits for them, and re-layouts: 39 us -> none  [the longest x2 17.9 us: body(): lax.all_to_all(down_cols, 'tp', split_axis=1, concat_axis=2, tiled=True)]
    all_to_all x6 -> x0, starting transfers between devices: 33.6 us -> none  [the longest x1 7.44 us: body(): lax.all_to_all(down_local, 'fs', split_axis=0, concat_axis=1, tiled=True)]
    unnamed x14, local copies, waits for them, and re-layouts: 16.8 us -> 29.1 us
    all_gather x1 -> x0, local copies, waits for them, and re-layouts: 12.1 us -> none  [body(): lax.all_gather(served[2], 'gr', axis=1, tiled=True)]
    scatter x1 -> x0, local copies, waits for them, and re-layouts: 7.81 us -> none  [body(): jnp.zeros((EXPERTS * CAP, normed.shape[1]), jnp.bfloat16).at[target_rows]]
  transfers between devices with their start and end apart: 10 -> 0, of which waited for: 7 -> 0; matrix products, arithmetic and copies ran while one was open for 12% -> 0% of each run, Pallas kernels for 0% -> 0%
where the time goes in v2:
time: 466 us; the launch traced here: 465 us
  Pallas kernels  388 us (83%)
  local copies, waits for them, and re-layouts  32.2 us (7%)
  matrix products  23.4 us (5%)
  other arithmetic  21.1 us (5%)
    pallas_call x1, Pallas kernels, body(): pl.pallas_call(exchange_kernel, out_shape=(jax.ShapeDtypeStruct((fs_n, ro...  335 us
    pallas_call x1, Pallas kernels, body(): pl.pallas_call(return_kernel, out_shape=jax.ShapeDtypeStruct((rows, half)...  52.3 us
    unnamed x14, local copies, waits for them, and re-layouts  29.1 us
    dot_general x1, matrix products, body(): jnp.einsum('erf,efd->erd', hidden, down_weight, preferred_element_type=jn...  14.2 us
    convert_element_type x1, other arithmetic, body(): up_local = (norm_gain[None, :, None] * up_train).astype(jnp.bfloat16)  11.9 us

profile of v2, /device:TPU:0, one launch (start us, length us, event | category | flops | bytes accessed | tf_op | source)
XLA Modules:
  0.0 465.2 jit_solution(5432663652683065191)
XLA Ops:
  0.6 11.9 %multiply_convert_fusion = (bf16[32,128,512]{2,1,0:T(8,128)(2,1)}, bf16[32,128,512]{2,1,0:T(8,128)(2,1)}) fusion(f32[32,128,512]{2,1,0:T(8,128)} %param.10, f32[128]{0:T(128)} %param.8, f32[32,128,512]{2,1,0:T(8,128)} %param.9), kind=kLoop, calls=%fused_computation | loop fusion | flops 8388608 | bytes 25166336 | tf_op jit(solution)/shard_map/convert_element_type | solution.py:309
  12.5 6.1 %convert_element_type.48.down = bf16[32,64,1024]{2,1,0:T(8,128)(2,1)} convert(f32[32,64,1024]{2,1,0:T(8,128)} %param.11) | non-fusion elementwise | flops 2097152 | bytes 12582912 | tf_op jit(solution)/shard_map/convert_element_type | solution.py:310
  18.7 0.2 fusion.2
  18.9 1.0 fusion.3.normed
  19.9 0.6 pad_maximum_fusion.routing
  20.5 335.5 %shard_map.102 = (bf16[8,128,2048]{2,1,0:T(8,128)(2,1)}, f32[8,8,128]{2,1,0:T(8,128)}, bf16[4,2048,512]{2,1,0:T(8,128)(2,1)}, bf16[4,2048,512]{2,1,0:T(8,128)(2,1)}, bf16[4,512,2048]{2,1,0:T(8,128)(2,1)}) custom-call(bf16[128,2048]{1,0:T(8,128)(2,1)} %fusion.3.normed, f32[8,128]{1,0:T(8,128)} %pad_maximum_fusion.routing, ...), custom_call_target="tpu_custom_call" | custom-call | tf_op jit(solution)/shard_map/pallas_call | solution.py:320
  356.0 0.8 slice_convert_fusion
  356.8 0.1 compare_reduce_fusion
  356.9 0.1 fusion.1
  357.1 0.1 eq.40
  357.1 0.1 bitcast_compare_fusion
  357.3 3.4 convolution_convert_fusion.2
  360.7 0.6 copy.30
  361.3 4.3 copy-done
  365.6 2.3 fusion.12
  368.0 14.2 %convolution_convert_fusion = bf16[4,256,2048]{2,1,0:T(8,128)(2,1)} fusion(bf16[4,512,2048]{2,1,0:T(8,128)(2,1)} %get-tuple-element.25, f32[4,256,512]{2,1,0:T(8,128)S(1)} %fusion.12, bf16[4,256,2048]{2,1,0:T(8,128)(2,1)} %bitcast.35, bf16[4,2048,512]{2,1,0:T(8,128)(2,1)} %get-tuple-element.24), kind=kOutput, calls=%fused_computation.2 | convolution fusion | flops 4302307328 | bytes 27262976 | tf_op jit(solution)/shard_map/erf,efd->erd/dot_general | solution.py:374
  382.1 2.5 copy.31
  384.7 0.1 fusion.4
  384.8 3.3 convolution_convert_fusion.1.partial_mix
  388.2 52.3 %shard_map.103 = bf16[128,1024]{1,0:T(8,128)(2,1)} custom-call(bf16[8,128,2048]{2,1,0:T(8,128)(2,1)} %convolution_convert_fusion.1.partial_mix), custom_call_target="tpu_custom_call" | custom-call | tf_op jit(solution)/shard_map/pallas_call | solution.py:388
  440.5 1.7 copy.40
  442.1 7.3 %copy.41 = bf16[4,2048,512]{2,1,0:T(8,128)(2,1)} copy(bf16[4,2048,512]{2,1,0:T(8,128)(2,1)} %get-tuple-element.23) | data formatting | bytes 16777216
  449.5 7.3 %copy.42 = bf16[4,2048,512]{2,1,0:T(8,128)(2,1)} copy(bf16[4,2048,512]{2,1,0:T(8,128)(2,1)} %get-tuple-element.24) | data formatting | bytes 16777216
  456.8 8.4 %copy.43 = bf16[4,512,2048]{2,1,0:T(8,128)(2,1)} copy(bf16[4,512,2048]{2,1,0:T(8,128)(2,1)} %get-tuple-element.25) | data formatting | bytes 16777216
  (18 shorter events, 0.1 us)
Async XLA Ops:
  12.5 6.1 %copy-start.2 = (bf16[128,2048]{1,0:T(8,128)(2,1)S(1)}, bf16[128,2048]{1,0:T(8,128)(2,1)}, u32[]{:S(2)}) copy-start(bf16[128,2048]{1,0:T(8,128)(2,1)} %param.7) | copy-start | bytes 1572868
  12.5 7.3 %copy-start.3 = (s32[128,4]{0,1:T(4,128)S(1)}, s32[128,4]{0,1:T(4,128)}, u32[]{:S(2)}) copy-start(s32[128,4]{0,1:T(4,128)} %param.12) | copy-start | bytes 6148
  12.5 7.3 %copy-start.4 = (f32[128,4]{0,1:T(4,128)S(1)}, f32[128,4]{0,1:T(4,128)}, u32[]{:S(2)}) copy-start(f32[128,4]{0,1:T(4,128)} %param.13) | copy-start | bytes 6148
  360.7 4.9 %copy-start = (bf16[4,2048,512]{2,1,0:T(8,128)(2,1)S(1)}, bf16[4,2048,512]{2,1,0:T(8,128)(2,1)}, u32[]{:S(2)}) copy-start(bf16[4,2048,512]{2,1,0:T(8,128)(2,1)} %get-tuple-element.23) | copy-start | bytes 25165828
  361.3 6.6 %copy-start.1 = (bf16[4,8,32,2048]{3,2,1,0:T(8,128)(2,1)}, bf16[4,8,32,2048]{3,2,1,0:T(8,128)(2,1)S(1)}, u32[]{:S(2)}) copy-start(bf16[4,8,32,2048]{3,2,1,0:T(8,128)(2,1)S(1)} %copy.30) | copy-start | bytes 12582916

commit v3 on v2

--- a/solution.py
+++ b/solution.py
@@ -13,6 +13,8 @@
 NORM_EPSILON = 1e-06
 MESH = pl.DeviceIdType.MESH
 STEPS = (2, 3, 1, 6, 7, 4, 5)
+OUTER = (2, 1, 3, 6, 7, 4, 5)
+INNER = (6, 2, 7, 3, 4, 1, 5)
 
 
 def plain_body(tokens, norm_gain, gate_train, up_train, down_train, routes, route_weight):
@@ -75,20 +77,16 @@
 
 def flip(fs, step):
     z, y = lax.div(fs, 2), lax.rem(fs, 2)
-    if step % 2:
-        y = 1 - y
-    if step // 2 == 3:
-        z = 3 - z
-    elif step // 2 == 2:
-        z = lax.rem(z + 2, 4)
-    elif step // 2 == 1:
-        z = z + 1 - 2 * lax.rem(z, 2)
-    return z * 2 + y
+    turn = lax.div(step, 2) if not isinstance(step, int) else step // 2
+    low = lax.rem(lax.rem(z, 2) + turn, 2)
+    high = lax.rem(lax.div(z, 2) + (turn // 2 if isinstance(turn, int) else lax.div(turn, 2)), 2)
+    return (high * 2 + low) * 2 + lax.rem(y + step, 2)
 
 
 def exchange_kernel(
-    normed, routing, gate, up, down,
+    normed, routing, gain, gate, up, down,
     normed_all, routing_all, gate_out, up_out, down_out,
+    gate_half, up_half, down_half, gate_stage, up_stage, down_stage, load_sem,
     send, recv, relay_send, relay_recv, local_sem, tok_send, tok_recv, route_send, route_recv,
 ):
     g, f, t = lax.axis_index("gr"), lax.axis_index("fs"), lax.axis_index("tp")
@@ -144,26 +142,54 @@
 
     partner = (1 - g, f, t)
     keep = [
-        pltpu.make_async_copy(part(gate, f), gate_at(gate_out, g, f), local_sem.at[0]),
-        pltpu.make_async_copy(part(up, f), gate_at(up_out, g, f), local_sem.at[1]),
         pltpu.make_async_copy(normed, normed_all.at[f], local_sem.at[2]),
         pltpu.make_async_copy(routing, routing_all.at[f], local_sem.at[3]),
     ]
+    for copy in keep:
+        copy.start()
+
+    inner = lax.rem(lax.div(lax.div(f, 2) + 1, 2), 2)
+    order = [a + inner * (b - a) for a, b in zip(OUTER, INNER)] + [0]
+    stages, halves = (gate_stage, up_stage, down_stage), (gate_half, up_half, down_half)
+
+    def load(position, which):
+        there = flip(f, order[position])
+        return pltpu.make_async_copy(
+            part((gate, up, down)[which], there),
+            stages[which].at[position % 2],
+            load_sem.at[which, position % 2],
+        )
+
     main = {}
-    for s in STEPS:
-        there = flip(f, s)
-        main[0, s] = remote(part(gate, there), gate_at(gate_out, g, f), send.at[0, s],
-                            recv.at[0, s], (g, there, t))
-        main[1, s] = remote(part(up, there), gate_at(up_out, g, f), send.at[1, s],
-                            recv.at[1, s], (g, there, t))
-        main[2, s] = remote(part(down, there), down_at(f, t), send.at[2, s], recv.at[2, s],
-                            (t, there, g))
-    turn = remote(part(down, f), down_at(f, t), send.at[2, 0], recv.at[2, 0], (1 - g, f, 1 - t))
-    stay = pltpu.make_async_copy(part(down, f), down_at(f, t), local_sem.at[4])
-
-    for s in STEPS:
+    relays = {}
+    for which in range(3):
+        load(0, which).start()
+    for position, step in enumerate(order):
+        there = flip(f, step)
         for which in range(3):
-            main[which, s].start()
+            if position + 1 < len(order):
+                load(position + 1, which).start()
+            load(position, which).wait()
+            stage, halved = stages[which], halves[which]
+
+            @pl.loop(0, local_experts)
+            def _(e):
+                wide_block = stage[position % 2, e]
+                if which < 2:
+                    wide_block = gain[...] * wide_block
+                halved[position, e] = wide_block.astype(jnp.bfloat16)
+
+            if position + 1 < len(order):
+                target = (t, there, g) if which == 2 else (g, there, t)
+                place = down_at(f, t) if which == 2 else gate_at((gate_out, up_out)[which], g, f)
+                main[which, position] = remote(
+                    halved.at[position], place, send.at[which, step], recv.at[which, step], target
+                )
+                main[which, position].start()
+    last = len(order) - 1
+    turn = remote(down_half.at[last], down_at(f, t), send.at[2, 0], recv.at[2, 0],
+                  (1 - g, f, 1 - t))
+    stay = pltpu.make_async_copy(down_half.at[last], down_at(f, t), local_sem.at[4])
 
     @pl.when(g != t)
     def _():
@@ -173,16 +199,13 @@
     def _():
         stay.start()
 
-    for copy in keep:
-        copy.start()
-
-    relays = {}
-    relays[0, 0] = remote(part(gate, f), gate_at(gate_out, g, f), relay_send.at[0, 0],
-                          relay_recv.at[0, 0], partner)
-    relays[1, 0] = remote(part(up, f), gate_at(up_out, g, f), relay_send.at[1, 0],
-                          relay_recv.at[1, 0], partner)
-    relays[0, 0].start()
-    relays[1, 0].start()
+    for which in range(2):
+        place = gate_at((gate_out, up_out)[which], g, f)
+        keep.append(pltpu.make_async_copy(halves[which].at[last], place, local_sem.at[which]))
+        keep[-1].start()
+        relays[which, 0] = remote(halves[which].at[last], place, relay_send.at[which, 0],
+                                  relay_recv.at[which, 0], partner)
+        relays[which, 0].start()
 
     across = (g, flip(f, 1), t)
     second = {0: remote(own_half, tok(f), tok_send.at[1], tok_recv.at[1], across)}
@@ -215,20 +238,21 @@
     for s in STEPS:
         source = flip(f, s)
         for which in range(3):
-            main[which, s].wait_recv()
             if which == 2:
                 block = down_at(source, g)
             else:
                 block = gate_at((gate_out, up_out)[which], g, source)
+            remote(halves[which].at[0], block, send.at[which, s], recv.at[which, s],
+                   partner).wait_recv()
             relays[which, s] = remote(block, block, relay_send.at[which, s],
                                       relay_recv.at[which, s], partner)
             relays[which, s].start()
     for s in (0,) + STEPS:
         for which in range(3):
             relays[which, s].wait()
+    for copy in main.values():
+        copy.wait_send()
     for s in STEPS:
-        for which in range(3):
-            main[which, s].wait_send()
         small[s].wait()
         third[s].wait()
     for s in (2, 4, 6):
@@ -299,15 +323,31 @@
             copies[i, q].wait_send()
 
 
+def expert_kernel(arrived, gate, up, down, results, gate_out, up_out, down_out):
+    gate_out[...] = gate[...]
+    up_out[...] = up[...]
+    down_out[...] = down[...]
+    rows = arrived[...]
+    gate_pre = jnp.dot(rows, gate[...], preferred_element_type=jnp.float32)
+    up_pre = jnp.dot(rows, up[...], preferred_element_type=jnp.float32)
+    clipped = jnp.minimum(gate_pre, CLAMP_LIMIT)
+    hidden = (
+        (jnp.clip(up_pre, -CLAMP_LIMIT, CLAMP_LIMIT) + 1.0)
+        * clipped
+        * jax.nn.sigmoid(SLOPE_ALPHA * clipped)
+    ).astype(jnp.bfloat16)
+    results[...] = jnp.dot(hidden, down[...], preferred_element_type=jnp.float32).astype(
+        jnp.bfloat16
+    )
+
+
 def body(tokens, norm_gain, gate_train, up_train, down_train, routes, route_weight):
     fs_n = 8
     experts, rows_in, hidden_part = gate_train.shape
     local_experts = experts // fs_n
     rows, width = tokens.shape
     top = routes.shape[1]
-    gate_local = (norm_gain[None, :, None] * gate_train).astype(jnp.bfloat16)
-    up_local = (norm_gain[None, :, None] * up_train).astype(jnp.bfloat16)
-    down_local = down_train.astype(jnp.bfloat16)
+    gain = jnp.broadcast_to(norm_gain[:, None], (rows_in, hidden_part))
     tokens_wide = tokens.astype(jnp.float32)
     normed = (
         tokens_wide
@@ -328,14 +368,21 @@
                 (local_experts, down_train.shape[1] * fs_n, down_train.shape[2] * 2), jnp.bfloat16
             ),
         ),
-        in_specs=[anywhere] * 5,
+        in_specs=[anywhere] * 2 + [pl.BlockSpec(memory_space=pltpu.VMEM)] + [anywhere] * 3,
         out_specs=(anywhere,) * 5,
         scratch_shapes=[
+            pltpu.VMEM((fs_n, local_experts) + gate_train.shape[1:], jnp.bfloat16),
+            pltpu.VMEM((fs_n, local_experts) + up_train.shape[1:], jnp.bfloat16),
+            pltpu.VMEM((fs_n, local_experts) + down_train.shape[1:], jnp.bfloat16),
+            pltpu.VMEM((2, local_experts) + gate_train.shape[1:], jnp.float32),
+            pltpu.VMEM((2, local_experts) + up_train.shape[1:], jnp.float32),
+            pltpu.VMEM((2, local_experts) + down_train.shape[1:], jnp.float32),
+            dma((3, 2)),
             dma((3, 8)), dma((3, 8)), dma((3, 8)), dma((3, 8)), dma((5,)),
             dma((16,)), dma((16,)), dma((8,)), dma((8,)),
         ],
         compiler_params=pltpu.CompilerParams(collective_id=0, has_side_effects=True),
-    )(normed, routing, gate_local, up_local, down_local)
+    )(normed, routing, gain, gate_train, up_train, down_train)
 
     routes_all = routing_all[:, :top].astype(jnp.int32)
     weight_all = routing_all[:, top:]
@@ -363,17 +410,17 @@
         .transpose(1, 0, 2, 3)
         .reshape(local_experts, fs_n * CAP, width)
     )
-    gate_pre = jnp.einsum("erd,edf->erf", arrived, gate_weight, preferred_element_type=jnp.float32)
-    up_pre = jnp.einsum("erd,edf->erf", arrived, up_weight, preferred_element_type=jnp.float32)
-    clipped = jnp.minimum(gate_pre, CLAMP_LIMIT)
-    hidden = (
-        (jnp.clip(up_pre, -CLAMP_LIMIT, CLAMP_LIMIT) + 1.0)
-        * clipped
-        * jax.nn.sigmoid(SLOPE_ALPHA * clipped)
-    ).astype(jnp.bfloat16)
-    results = jnp.einsum(
-        "erf,efd->erd", hidden, down_weight, preferred_element_type=jnp.float32
-    ).astype(jnp.bfloat16)
+    def block(array):
+        return pl.BlockSpec((None,) + array.shape[1:], lambda e: (e, 0, 0))
+
+    weights = (gate_weight, up_weight, down_weight)
+    results, gate_weight, up_weight, down_weight = pl.pallas_call(
+        expert_kernel,
+        grid=(local_experts,),
+        out_shape=[jax.ShapeDtypeStruct(a.shape, jnp.bfloat16) for a in (arrived,) + weights],
+        in_specs=[block(a) for a in (arrived,) + weights],
+        out_specs=[block(a) for a in (arrived,) + weights],
+    )(arrived, *weights)
     results = (
         results.reshape(local_experts, fs_n, CAP, width)
         .transpose(1, 0, 2, 3)

time: 466 us -> 432 us (0.927)
  local copies, waits for them, and re-layouts: 32.2 us -> 8 us
  Pallas kernels: 388 us -> 409 us
  matrix products: 23.4 us -> 6.79 us
  other arithmetic: 21.1 us -> 6.46 us
    unnamed x14 -> x1, local copies, waits for them, and re-layouts: 29.1 us -> 1.67 us
    pallas_call x0 -> x1, Pallas kernels: none -> 20.5 us  [body(): pl.pallas_call(expert_kernel, grid=(local_experts,), out_shape=[jax.Shape...]
    convert_element_type x2 -> x0, other arithmetic: 18 us -> none  [the longest x1 11.9 us: body(): up_local = (norm_gain[None, :, None] * up_train).astype(jnp.bfloat16)]
    dot_general x2 -> x0, matrix products: 16.5 us -> none  [the longest x1 14.2 us: body(): jnp.einsum('erf,efd->erd', hidden, down_weight, preferred_element_type=jn...]
where the time goes in v3:
time: 432 us; the launch traced here: 431 us
  Pallas kernels  409 us (95%)
  local copies, waits for them, and re-layouts  8 us (2%)
  matrix products  6.79 us (2%)
  other arithmetic  6.46 us (1%)
    pallas_call x1, Pallas kernels, body(): pl.pallas_call(exchange_kernel, out_shape=(jax.ShapeDtypeStruct((fs_n, ro...  336 us
    pallas_call x1, Pallas kernels, body(): pl.pallas_call(return_kernel, out_shape=jax.ShapeDtypeStruct((rows, half)...  52.3 us
    pallas_call x1, Pallas kernels, body(): pl.pallas_call(expert_kernel, grid=(local_experts,), out_shape=[jax.Shape...  20.5 us

profile of v3, /device:TPU:0, one launch (start us, length us, event | category | flops | bytes accessed | tf_op | source)
XLA Modules:
  0.0 431.0 jit_solution(8158532398023080516)
XLA Ops:
  0.6 1.2 fusion.2
  1.9 0.7 convert_bitcast_fusion
  2.6 1.3 pad_maximum_fusion.routing
  3.9 0.1 eq.40
  3.9 1.4 broadcast_in_dim.26.gain
  5.4 2.0 fusion.3.normed
  7.4 336.2 %shard_map.102 = (bf16[8,128,2048]{2,1,0:T(8,128)(2,1)}, f32[8,8,128]{2,1,0:T(8,128)}, bf16[4,2048,512]{2,1,0:T(8,128)(2,1)}, bf16[4,2048,512]{2,1,0:T(8,128)(2,1)}, bf16[4,512,2048]{2,1,0:T(8,128)(2,1)}) custom-call(bf16[128,2048]{1,0:T(8,128)(2,1)} %fusion.3.normed, f32[8,128]{1,0:T(8,128)} %pad_maximum_fusion.routing, f32[128,512]{1,0:T(8,128)} %broadcast_in_dim.26.gain, ...), custom_call_target="tpu_custom_call" | custom-call | tf_op jit(solution)/shard_map/pallas_call | solution.py:360
  343.6 0.8 slice_convert_fusion
  344.4 0.1 compare_reduce_fusion
  344.5 0.1 fusion.1
  344.7 0.1 fusion.5
  344.8 0.1 bitcast_compare_fusion
  344.9 3.4 convolution_convert_fusion.1
  348.3 2.3 copy.30
  350.6 20.5 %shard_map.103 = (bf16[4,256,2048]{2,1,0:T(8,128)(2,1)}, bf16[4,2048,512]{2,1,0:T(8,128)(2,1)}, bf16[4,2048,512]{2,1,0:T(8,128)(2,1)}, bf16[4,512,2048]{2,1,0:T(8,128)(2,1)}) custom-call(bf16[4,256,2048]{2,1,0:T(8,128)(2,1)} %bitcast.27, bf16[4,2048,512]{2,1,0:T(8,128)(2,1)} %get-tuple-element.15.gate, bf16[4,2048,512]{2,1,0:T(8,128)(2,1)} %get-tuple-element.16.up, ...), custom_call_target="tpu_custom_call" | custom-call | tf_op jit(solution)/shard_map/pallas_call | solution.py:417
  371.2 2.5 copy.31
  373.7 0.1 fusion.4
  373.8 3.2 convolution_convert_fusion.partial_mix
  377.0 52.3 %shard_map.104 = bf16[128,1024]{1,0:T(8,128)(2,1)} custom-call(bf16[8,128,2048]{2,1,0:T(8,128)(2,1)} %convolution_convert_fusion.partial_mix), custom_call_target="tpu_custom_call" | custom-call | tf_op jit(solution)/shard_map/pallas_call | solution.py:435
  429.3 1.7 copy.37
  (7 shorter events, 0.0 us)

commit v4 on v3

--- a/solution.py
+++ b/solution.py
@@ -13,8 +13,8 @@
 NORM_EPSILON = 1e-06
 MESH = pl.DeviceIdType.MESH
 STEPS = (2, 3, 1, 6, 7, 4, 5)
-OUTER = (2, 1, 3, 6, 7, 4, 5)
-INNER = (6, 2, 7, 3, 4, 1, 5)
+OUTER = (6, 2, 7, 3, 4, 1, 5)
+INNER = (4, 2, 5, 3, 6, 1, 7)
 
 
 def plain_body(tokens, norm_gain, gate_train, up_train, down_train, routes, route_weight):

time: 432 us -> 407 us (0.942)
  Pallas kernels: 409 us -> 384 us
    pallas_call x1, Pallas kernels: 336 us -> 239 us  [body(): pl.pallas_call(exchange_kernel, out_shape=(jax.ShapeDtypeStruct((fs_n, ro...]
    pallas_call x1, Pallas kernels: 52.3 us -> 125 us  [body(): pl.pallas_call(return_kernel, out_shape=jax.ShapeDtypeStruct((rows, half)...]
where the time goes in v4:
time: 407 us; the launch traced here: 406 us
  Pallas kernels  384 us (94%)
  local copies, waits for them, and re-layouts  8 us (2%)
  matrix products  6.79 us (2%)
  other arithmetic  6.46 us (2%)
    pallas_call x1, Pallas kernels, body(): pl.pallas_call(exchange_kernel, out_shape=(jax.ShapeDtypeStruct((fs_n, ro...  239 us
    pallas_call x1, Pallas kernels, body(): pl.pallas_call(return_kernel, out_shape=jax.ShapeDtypeStruct((rows, half)...  125 us
    pallas_call x1, Pallas kernels, body(): pl.pallas_call(expert_kernel, grid=(local_experts,), out_shape=[jax.Shape...  20.5 us

profile of v4, /device:TPU:0, one launch (start us, length us, event | category | flops | bytes accessed | tf_op | source)
XLA Modules:
  0.0 406.4 jit_solution(7303601246607492041)
XLA Ops:
  0.6 1.2 fusion.2
  1.9 0.7 convert_bitcast_fusion
  2.6 1.3 pad_maximum_fusion.routing
  3.9 0.1 eq.40
  3.9 1.4 broadcast_in_dim.26.gain
  5.4 2.0 fusion.3.normed
  7.4 238.5 %shard_map.102 = (bf16[8,128,2048]{2,1,0:T(8,128)(2,1)}, f32[8,8,128]{2,1,0:T(8,128)}, bf16[4,2048,512]{2,1,0:T(8,128)(2,1)}, bf16[4,2048,512]{2,1,0:T(8,128)(2,1)}, bf16[4,512,2048]{2,1,0:T(8,128)(2,1)}) custom-call(bf16[128,2048]{1,0:T(8,128)(2,1)} %fusion.3.normed, f32[8,128]{1,0:T(8,128)} %pad_maximum_fusion.routing, f32[128,512]{1,0:T(8,128)} %broadcast_in_dim.26.gain, ...), custom_call_target="tpu_custom_call" | custom-call | tf_op jit(solution)/shard_map/pallas_call | solution.py:360
  245.9 0.8 slice_convert_fusion
  246.8 0.1 compare_reduce_fusion
  246.8 0.1 fusion.1
  247.0 0.1 fusion.5
  247.1 0.1 bitcast_compare_fusion
  247.2 3.4 convolution_convert_fusion.1
  250.7 2.3 copy.30
  253.0 20.5 %shard_map.103 = (bf16[4,256,2048]{2,1,0:T(8,128)(2,1)}, bf16[4,2048,512]{2,1,0:T(8,128)(2,1)}, bf16[4,2048,512]{2,1,0:T(8,128)(2,1)}, bf16[4,512,2048]{2,1,0:T(8,128)(2,1)}) custom-call(bf16[4,256,2048]{2,1,0:T(8,128)(2,1)} %bitcast.27, bf16[4,2048,512]{2,1,0:T(8,128)(2,1)} %get-tuple-element.15.gate, bf16[4,2048,512]{2,1,0:T(8,128)(2,1)} %get-tuple-element.16.up, ...), custom_call_target="tpu_custom_call" | custom-call | tf_op jit(solution)/shard_map/pallas_call | solution.py:417
  273.5 2.5 copy.31
  276.0 0.1 fusion.4
  276.1 3.2 convolution_convert_fusion.partial_mix
  279.4 125.4 %shard_map.104 = bf16[128,1024]{1,0:T(8,128)(2,1)} custom-call(bf16[8,128,2048]{2,1,0:T(8,128)(2,1)} %convolution_convert_fusion.partial_mix), custom_call_target="tpu_custom_call" | custom-call | tf_op jit(solution)/shard_map/pallas_call | solution.py:435
  404.7 1.7 copy.37
  (7 shorter events, 0.0 us)
